TPU v7x, 32 devices: a whole 2x2x4 slice. The times are simulated.
32 devices in a mesh: rep: 2 (over y), fs: 4 (over z), tp: 4 (over x, core).
Axes of the slice: x: 2, y: 2, z: 4, core: 2. Of those that a mesh axis runs over, the one named last changes fastest.
Arguments:
- stream: bfloat16 [4096, 2048], P(('rep', 'fs', 'tp')), may hold values from -6 to 6
- gain_before: float32 [2048], replicated, may hold values from 0.1 to 1.9
- gain_after: float32 [2048], replicated, may hold values from 0.1 to 1.9
- proj_gate: bfloat16 [2048, 3584], P('fs', 'tp'), may hold values from -0.125 to 0.125
- proj_lift: bfloat16 [2048, 3584], P('fs', 'tp'), may hold values from -0.125 to 0.125
- proj_down: bfloat16 [3584, 2048], P('tp', 'fs'), may hold values from -0.09375 to 0.09375
- mixer_gain: float32 [2048], replicated, may hold values from 0.1 to 1.9
- mixer_u: bfloat16 [2048, 2048], P('fs', 'tp'), may hold values from -0.125 to 0.125
- mixer_v: bfloat16 [2048, 2048], P('fs', 'tp'), may hold values from -1 to 1
- layer_gain: float32 [2048], P('tp'), may hold values from 0.1 to 1.9
- layer_shift: float32 [2048], P('tp'), may hold values from -3 to 3
- spatial: bfloat16 [16, 128, 128], P('tp'), may hold values from -0.5 to 0.5
- spatial_shift: float32 [16, 128], P('tp'), may hold values from 0.2 to 2
- mixer_down: bfloat16 [2048, 2048], P('tp', 'fs'), may hold values from -0.125 to 0.125
Outputs:
- result: bfloat16 [4096, 2048], P(('rep', 'fs', 'tp'))
All inputs are finite; a program needn't handle non-finite values.
Results may differ from a plain program's by a relative error of at most 0.017.
Values may be sent and summed in bfloat16 or wider, within the bound.
A program may use at most 128 MiB of HBM per device.

v0:
```python
import jax
import jax.numpy as jnp
from jax import lax
from jax.sharding import PartitionSpec as P

GROUP_DIM = 128
SPAN = 128
A = 2048
norm_epsilon = 1e-06
layer_epsilon = 1e-05


def norm_rows(row_block, scale_gain):
    widened = row_block.astype(jnp.float32)
    factor = lax.rsqrt(jnp.mean(widened * widened, axis=1, keepdims=True) + norm_epsilon)
    return (widened * factor * scale_gain).astype(jnp.bfloat16)


def gathered_norm(stream_rows, scale_gain):
    gathered = lax.all_gather(stream_rows, "tp", axis=0, tiled=True)
    return norm_rows(gathered, scale_gain)


def pair_adder(normed, pieces):
    return (
        jnp.dot(normed, pieces[0], preferred_element_type=jnp.float32),
        jnp.dot(normed, pieces[1], preferred_element_type=jnp.float32),
    )


def activate(gate_vals, lift_vals):
    return (jax.nn.silu(gate_vals) * lift_vals).astype(jnp.bfloat16)


def half_again(stream_rows, scale_gain, proj_gate, proj_lift, proj_down):
    normed = gathered_norm(stream_rows, scale_gain)
    gate_vals, lift_vals = pair_adder(
        normed,
        (
            lax.all_gather(proj_gate, "fs", axis=0, tiled=True),
            lax.all_gather(proj_lift, "fs", axis=0, tiled=True),
        ),
    )
    hidden = activate(gate_vals, lift_vals)
    partial_value = jnp.dot(
        hidden,
        lax.all_gather(proj_down, "fs", axis=1, tiled=True),
        preferred_element_type=jnp.float32,
    )
    summed = lax.psum_scatter(
        partial_value.astype(jnp.bfloat16), "tp", scatter_dimension=0, tiled=True
    ).astype(jnp.float32)
    return (stream_rows.astype(jnp.float32) + 0.5 * summed).astype(jnp.bfloat16)


def token_mixer(
    stream_rows,
    mixer_gain,
    mixer_u,
    mixer_v,
    layer_gain,
    layer_shift,
    spatial,
    spatial_shift,
    mixer_down,
):
    gathered = lax.all_gather(stream_rows, "tp", axis=0, tiled=True)
    normed = norm_rows(gathered, mixer_gain)
    seq_tokens = normed.shape[0]
    u_vals, v_vals = pair_adder(
        normed,
        (
            lax.all_gather(mixer_u, "fs", axis=0, tiled=True),
            lax.all_gather(mixer_v, "fs", axis=0, tiled=True),
        ),
    )
    lifted = jax.nn.gelu(v_vals)
    moments = lax.psum((jnp.sum(lifted, axis=1), jnp.sum(lifted * lifted, axis=1)), "tp")
    centre = moments[0] / A
    spread = moments[1] / A - centre * centre
    normed_v = (
        (lifted - centre[:, None]) * lax.rsqrt(spread[:, None] + layer_epsilon) * layer_gain
        + layer_shift
    ).astype(jnp.bfloat16)
    groups_here = spatial.shape[0]
    blocked = normed_v.reshape(seq_tokens // SPAN, SPAN, groups_here, GROUP_DIM)
    causal = jnp.tril(jnp.ones((SPAN, SPAN), dtype=bool))
    masked = jnp.where(causal[None], spatial, jnp.zeros((), jnp.bfloat16))
    mixed_v = jnp.einsum("gts,bsgd->btgd", masked, blocked, preferred_element_type=jnp.float32)
    mixed_v = mixed_v + spatial_shift.T[None, :, :, None]
    gated = (jax.nn.gelu(u_vals) * mixed_v.reshape(seq_tokens, groups_here * GROUP_DIM)).astype(
        jnp.bfloat16
    )
    partial_value = jnp.dot(
        gated,
        lax.all_gather(mixer_down, "fs", axis=1, tiled=True),
        preferred_element_type=jnp.float32,
    )
    summed = lax.psum_scatter(
        partial_value.astype(jnp.bfloat16), "tp", scatter_dimension=0, tiled=True
    ).astype(jnp.float32)
    return (stream_rows.astype(jnp.float32) + summed).astype(jnp.bfloat16)


def body(
    stream,
    gain_before,
    gain_after,
    proj_gate,
    proj_lift,
    proj_down,
    mixer_gain,
    mixer_u,
    mixer_v,
    layer_gain,
    layer_shift,
    spatial,
    spatial_shift,
    mixer_down,
):
    first = half_again(stream, gain_before, proj_gate, proj_lift, proj_down)
    second = token_mixer(
        first,
        mixer_gain,
        mixer_u,
        mixer_v,
        layer_gain,
        layer_shift,
        spatial,
        spatial_shift,
        mixer_down,
    )
    result = half_again(second, gain_after, proj_gate, proj_lift, proj_down)
    return result


def solution(mesh):
    placed = (
        P(("rep", "fs", "tp"), None),
        P(),
        P(),
        P("fs", "tp"),
        P("fs", "tp"),
        P("tp", "fs"),
        P(),
        P("fs", "tp"),
        P("fs", "tp"),
        P("tp"),
        P("tp"),
        P("tp", None, None),
        P("tp", None),
        P("tp", "fs"),
    )
    return jax.shard_map(
        body, mesh=mesh, in_specs=placed, out_specs=P(("rep", "fs", "tp"), None), check_vma=False
    )
```

profile of v0, /device:TPU:0, one launch (start us, length us, event | category | flops | bytes accessed | tf_op | source)
XLA Modules:
  0.0 575.2 jit_solution(15976335767558670113)
XLA Ops:
  6.5 0.0 all-gather.10.cloned.1.call-start
  6.5 0.7 all-gather.10.cloned.1.call-update
  7.3 0.0 all-gather.12.cloned.1.call-start
  7.3 0.7 all-gather.12.cloned.1.call-update
  8.0 0.0 copy-start.10
  8.0 0.0 all-gather.14.cloned.1.call-start
  8.1 0.7 all-gather.14.cloned.1.call-update
  8.8 0.0 all-gather.16.cloned.1.call-start
  8.8 0.5 all-gather.16.cloned.1.call-update
  9.3 0.0 reduce-scatter.4.cloned.1.call-start
  9.4 24.8 %all-gather.10.cloned.1.call-done = bf16[512,2048]{1,0:T(8,128)(2,1)} async-done(((bf16[128,2048]{1,0:T(8,128)(2,1)}), bf16[512,2048]{1,0:T(8,128)(2,1)}) %all-gather.10.cloned.1.call-update) | async-done | bytes 2097168 | tf_op jit(solution)/shard_map/all_gather | solution.py:20
  34.2 2.2 fusion
  36.4 71.5 %all-gather.12.cloned.1.call-done = bf16[2048,896]{1,0:T(8,128)(2,1)} async-done(((bf16[512,896]{1,0:T(8,128)(2,1)}), bf16[2048,896]{1,0:T(8,128)(2,1)}) %all-gather.12.cloned.1.call-update) | async-done | bytes 3670032 | tf_op jit(solution)/shard_map/all_gather | solution.py:40
  107.9 0.0 copy-done.10
  107.9 0.0 copy-done.4
  107.9 5.6 fusion.42
  113.5 66.6 %all-gather.14.cloned.1.call-done = bf16[2048,896]{1,0:T(8,128)(2,1)} async-done(((bf16[512,896]{1,0:T(8,128)(2,1)}), bf16[2048,896]{1,0:T(8,128)(2,1)}) %all-gather.14.cloned.1.call-update) | async-done | bytes 3670032 | tf_op jit(solution)/shard_map/all_gather | solution.py:41
  180.2 72.1 %all-gather.16.cloned.1.call-done = bf16[896,2048]{1,0:T(8,128)(2,1)} async-done(((bf16[896,512]{1,0:T(8,128)(2,1)}), bf16[896,2048]{1,0:T(8,128)(2,1)}) %all-gather.16.cloned.1.call-update) | async-done | bytes 3670032 | tf_op jit(solution)/shard_map/all_gather | solution.py:47
  252.3 9.7 %convolution_convert_fusion.1 = bf16[512,2048]{1,0:T(8,128)(2,1)} fusion(bf16[896,2048]{1,0:T(8,128)(2,1)} %all-gather.16.cloned.1.call-done, f32[512,896]{1,0:T(8,128)} %fusion.42, bf16[2048,896]{1,0:T(8,128)(2,1)} %all-gather.14.cloned.1.call-done, bf16[512,2048]{1,0:T(8,128)(2,1)S(1)} %copy-done.4, f32[2048]{0:T(1024)S(1)} %copy-done.10, ...), kind=kOutput, calls=%fused_computation.16 | convolution fusion | flops 3766091776 | bytes 13379584 | tf_op jit(solution)/shard_map/dot_general | solution.py:45
  262.0 0.0 reduce-scatter.4.cloned.1.call-update
  262.0 0.0 all-gather.18.cloned.1.call-start
  262.0 29.9 %reduce-scatter.4.cloned.1.call-done = bf16[128,2048]{1,0:T(8,128)(2,1)} async-done(((bf16[512,2048]{1,0:T(8,128)(2,1)}), bf16[128,2048]{1,0:T(8,128)(2,1)}) %reduce-scatter.4.cloned.1.call-update) | async-done | bytes 524304 | tf_op jit(solution)/shard_map/reduce_scatter | solution.py:50
  291.9 0.0 copy-done.2
  291.9 2.0 add_convert_fusion.3
  293.9 0.0 all-gather.18.cloned.1.call-update
  293.9 0.0 all-gather.22.cloned.1.call-start
  294.0 0.7 all-gather.22.cloned.1.call-update
  294.7 0.0 all-gather.20.cloned.1.call-start
  294.7 0.7 all-gather.20.cloned.1.call-update
  295.4 0.0 all-gather.24.cloned.1.call-start
  295.5 0.7 all-gather.24.cloned.1.call-update
  296.2 0.0 reduce-scatter.6.cloned.1.call-start
  296.2 20.4 %all-gather.18.cloned.1.call-done = bf16[512,2048]{1,0:T(8,128)(2,1)} async-done(((bf16[128,2048]{1,0:T(8,128)(2,1)}), bf16[512,2048]{1,0:T(8,128)(2,1)}) %all-gather.18.cloned.1.call-update) | async-done | bytes 2097168 | tf_op jit(solution)/shard_map/all_gather | solution.py:67
  316.6 2.2 fusion.3
  318.9 0.0 copy-start.7
  318.9 0.0 copy-start.8
  318.9 45.0 %all-gather.22.cloned.1.call-done = bf16[2048,512]{1,0:T(8,128)(2,1)} async-done(((bf16[512,512]{1,0:T(8,128)(2,1)}), bf16[2048,512]{1,0:T(8,128)(2,1)}) %all-gather.22.cloned.1.call-update) | async-done | bytes 2097168 | tf_op jit(solution)/shard_map/all_gather | solution.py:74
  363.9 0.0 copy-done.11
  363.9 0.0 copy-done.3
  363.9 4.1 fusion.60
  368.0 6.5 %all-reduce = (f32[512]{0:T(512)S(1)}, f32[512]{0:T(512)S(1)}) all-reduce(f32[512]{0:T(512)S(1)} %get-tuple-element.6, f32[512]{0:T(512)S(1)} %get-tuple-element.5), channel_id=1, replica_groups=mesh['rep'=2,'fs'=4,'tp'=4] {'tp'}, use_global_device_ids=true, to_apply=%region_6.7 | all-reduce | flops 1024 | bytes 8192 | tf_op jit(solution)/shard_map/psum | solution.py:78
  374.6 1.5 add_convert_fusion.2
  376.0 0.9 reshape.47
  377.0 0.0 copy-done.9
  377.0 1.4 fusion.9
  378.4 1.3 copy.21
  379.7 30.2 %all-gather.20.cloned.1.call-done = bf16[2048,512]{1,0:T(8,128)(2,1)} async-done(((bf16[512,512]{1,0:T(8,128)(2,1)}), bf16[2048,512]{1,0:T(8,128)(2,1)}) %all-gather.20.cloned.1.call-update) | async-done | bytes 2097168 | tf_op jit(solution)/shard_map/all_gather | solution.py:73
  409.9 46.1 %all-gather.24.cloned.1.call-done = bf16[512,2048]{1,0:T(8,128)(2,1)} async-done(((bf16[512,512]{1,0:T(8,128)(2,1)}), bf16[512,2048]{1,0:T(8,128)(2,1)}) %all-gather.24.cloned.1.call-update) | async-done | bytes 2097168 | tf_op jit(solution)/shard_map/all_gather | solution.py:96
  456.0 6.5 %convolution_convert_fusion.2 = bf16[512,2048]{1,0:T(8,128)(2,1)} fusion(bf16[512,2048]{1,0:T(8,128)(2,1)} %all-gather.24.cloned.1.call-done, f32[64,8,4,128]{3,2,1,0:T(4,128)} %bitcast.25, bf16[2048,512]{1,0:T(8,128)(2,1)} %all-gather.20.cloned.1.call-done, bf16[512,2048]{1,0:T(8,128)(2,1)S(1)} %copy-done.3, f32[2048]{0:T(1024)S(1)} %copy-done.11, ...), kind=kOutput, calls=%fused_computation.17 | convolution fusion | flops 2155347968 | bytes 9447424 | tf_op jit(solution)/shard_map/dot_general | solution.py:94
  462.5 0.0 reduce-scatter.6.cloned.1.call-update
  462.5 0.0 copy-start.12
  462.5 0.0 all-gather.26.cloned.1.call-start
  462.6 30.1 %reduce-scatter.6.cloned.1.call-done = bf16[128,2048]{1,0:T(8,128)(2,1)} async-done(((bf16[512,2048]{1,0:T(8,128)(2,1)}), bf16[128,2048]{1,0:T(8,128)(2,1)}) %reduce-scatter.6.cloned.1.call-update) | async-done | bytes 524304 | tf_op jit(solution)/shard_map/reduce_scatter | solution.py:99
  492.7 2.0 add_convert_fusion.1
  494.6 0.0 all-gather.26.cloned.1.call-update
  494.6 0.2 reduce-scatter.8.cloned.1.call-start
  494.9 22.5 %all-gather.26.cloned.1.call-done = bf16[512,2048]{1,0:T(8,128)(2,1)} async-done(((bf16[128,2048]{1,0:T(8,128)(2,1)}), bf16[512,2048]{1,0:T(8,128)(2,1)}) %all-gather.26.cloned.1.call-update) | async-done | bytes 2097168 | tf_op jit(solution)/shard_map/all_gather | solution.py:20
  517.4 2.2 fusion.6
  519.6 0.0 copy-done.12
  519.6 5.7 fusion.28
  525.3 9.7 %convolution_convert_fusion = bf16[512,2048]{1,0:T(8,128)(2,1)} fusion(bf16[896,2048]{1,0:T(8,128)(2,1)} %all-gather.16.cloned.1.call-done, f32[512,896]{1,0:T(8,128)} %fusion.28, bf16[2048,896]{1,0:T(8,128)(2,1)} %all-gather.14.cloned.1.call-done, bf16[512,2048]{1,0:T(8,128)(2,1)S(1)} %copy-done.5, f32[2048]{0:T(1024)S(1)} %copy-done.12, ...), kind=kOutput, calls=%fused_computation.15 | convolution fusion | flops 3766091776 | bytes 13379584 | tf_op jit(solution)/shard_map/dot_general | solution.py:45
  535.0 0.0 reduce-scatter.8.cloned.1.call-update
  535.0 31.3 %reduce-scatter.8.cloned.1.call-done = bf16[128,2048]{1,0:T(8,128)(2,1)} async-done(((bf16[512,2048]{1,0:T(8,128)(2,1)}), bf16[128,2048]{1,0:T(8,128)(2,1)}) %reduce-scatter.8.cloned.1.call-update) | async-done | bytes 524304 | tf_op jit(solution)/shard_map/reduce_scatter | solution.py:50
  566.4 2.0 add_convert_fusion
  (20 shorter events, 0.1 us)
Async XLA Ops:
  6.5 27.7 %all-gather.10.cloned.1.call-start = ((), (), s32[]{:S(2)}) async-start(), calls=%async_computation.3 | async-start | bytes 2621440 | tf_op jit(solution)/shard_map/all_gather | solution.py:20
  7.3 100.6 %all-gather.12.cloned.1.call-start = ((), (), s32[]{:S(2)}) async-start(), calls=%async_computation.4 | async-start | bytes 4587520 | tf_op jit(solution)/shard_map/all_gather | solution.py:40
  8.0 99.9 %copy-start.10 = (f32[2048]{0:T(1024)S(1)}, f32[2048]{0:T(1024)}, u32[]{:S(2)}) copy-start(f32[2048]{0:T(1024)} %param.15) | copy-start | bytes 24580
  8.0 172.2 %all-gather.14.cloned.1.call-start = ((), (), s32[]{:S(2)}) async-start(), calls=%async_computation.5 | async-start | bytes 4587520 | tf_op jit(solution)/shard_map/all_gather | solution.py:41
  8.8 243.5 %all-gather.16.cloned.1.call-start = ((), (), s32[]{:S(2)}) async-start(), calls=%async_computation.6 | async-start | bytes 4587520 | tf_op jit(solution)/shard_map/all_gather | solution.py:47
  9.3 282.6 %reduce-scatter.4.cloned.1.call-start = ((), (), s32[]{:S(2)}) async-start(), calls=%async_computation.7 | async-start | bytes 2621440 | tf_op jit(solution)/shard_map/reduce_scatter | solution.py:50
  34.2 73.7 %copy-start.4 = (bf16[512,2048]{1,0:T(8,128)(2,1)S(1)}, bf16[512,2048]{1,0:T(8,128)(2,1)}, u32[]{:S(2)}) copy-start(bf16[512,2048]{1,0:T(8,128)(2,1)} %all-gather.10.cloned.1.call-done) | copy-start | bytes 6291460
  262.0 29.9 %copy-start.2 = (bf16[128,2048]{1,0:T(8,128)(2,1)S(1)}, bf16[128,2048]{1,0:T(8,128)(2,1)}, u32[]{:S(2)}) copy-start(bf16[128,2048]{1,0:T(8,128)(2,1)} %param.14) | copy-start | bytes 1572868
  262.0 54.6 %all-gather.18.cloned.1.call-start = ((), (), s32[]{:S(2)}) async-start(), calls=%async_computation.8 | async-start | bytes 2621440 | tf_op jit(solution)/shard_map/all_gather | solution.py:67
  293.9 70.0 %copy-start.11 = (f32[2048]{0:T(1024)S(1)}, f32[2048]{0:T(1024)}, u32[]{:S(2)}) copy-start(f32[2048]{0:T(1024)} %param.20) | copy-start | bytes 24580
  293.9 70.0 %all-gather.22.cloned.1.call-start = ((), (), s32[]{:S(2)}) async-start(), calls=%async_computation.10 | async-start | bytes 2621440 | tf_op jit(solution)/shard_map/all_gather | solution.py:74
  294.7 115.3 %all-gather.20.cloned.1.call-start = ((), (), s32[]{:S(2)}) async-start(), calls=%async_computation.9 | async-start | bytes 2621440 | tf_op jit(solution)/shard_map/all_gather | solution.py:73
  295.4 160.6 %all-gather.24.cloned.1.call-start = ((), (), s32[]{:S(2)}) async-start(), calls=%async_computation.11 | async-start | bytes 2621440 | tf_op jit(solution)/shard_map/all_gather | solution.py:96
  296.2 196.5 %reduce-scatter.6.cloned.1.call-start = ((), (), s32[]{:S(2)}) async-start(), calls=%async_computation.12 | async-start | bytes 2621440 | tf_op jit(solution)/shard_map/reduce_scatter | solution.py:99
  316.6 47.3 %copy-start.3 = (bf16[512,2048]{1,0:T(8,128)(2,1)S(1)}, bf16[512,2048]{1,0:T(8,128)(2,1)}, u32[]{:S(2)}) copy-start(bf16[512,2048]{1,0:T(8,128)(2,1)} %all-gather.18.cloned.1.call-done) | copy-start | bytes 6291460
  318.9 55.7 %copy-start.7 = (f32[512]{0:T(512)S(1)}, f32[512]{0:T(512)}, u32[]{:S(2)}) copy-start(f32[512]{0:T(512)} %param.24) | copy-start | bytes 6148
  318.9 55.7 %copy-start.8 = (f32[512]{0:T(512)S(1)}, f32[512]{0:T(512)}, u32[]{:S(2)}) copy-start(f32[512]{0:T(512)} %param.23) | copy-start | bytes 6148
  368.0 8.9 %copy-start.6 = (bf16[4,128,128]{2,1,0:T(8,128)(2,1)S(1)}, bf16[4,128,128]{2,1,0:T(8,128)(2,1)}, u32[]{:S(2)}) copy-start(bf16[4,128,128]{2,1,0:T(8,128)(2,1)} %param.25) | copy-start | bytes 393220
  368.0 8.9 %copy-start.9 = (f32[4,128]{1,0:T(4,128)S(1)}, f32[4,128]{1,0:T(4,128)}, u32[]{:S(2)}) copy-start(f32[4,128]{1,0:T(4,128)} %param.26) | copy-start | bytes 6148
  462.5 30.2 %copy-start = (bf16[128,2048]{1,0:T(8,128)(2,1)S(1)}, bf16[128,2048]{1,0:T(8,128)(2,1)}, u32[]{:S(2)}) copy-start(bf16[128,2048]{1,0:T(8,128)(2,1)} %add_convert_fusion.3) | copy-start | bytes 1572868
  462.5 57.1 %copy-start.12 = (f32[2048]{0:T(1024)S(1)}, f32[2048]{0:T(1024)}, u32[]{:S(2)}) copy-start(f32[2048]{0:T(1024)} %param.16) | copy-start | bytes 24580
  462.5 54.8 %all-gather.26.cloned.1.call-start = ((), (), s32[]{:S(2)}) async-start(), calls=%async_computation.13 | async-start | bytes 2621440 | tf_op jit(solution)/shard_map/all_gather | solution.py:20
  494.6 71.7 %reduce-scatter.8.cloned.1.call-start = ((), (), s32[]{:S(2)}) async-start(), calls=%async_computation.14 | async-start | bytes 2621440 | tf_op jit(solution)/shard_map/reduce_scatter | solution.py:50
  517.4 2.2 copy-start.5
  535.0 31.4 %copy-start.1 = (bf16[128,2048]{1,0:T(8,128)(2,1)S(1)}, bf16[128,2048]{1,0:T(8,128)(2,1)}, u32[]{:S(2)}) copy-start(bf16[128,2048]{1,0:T(8,128)(2,1)} %add_convert_fusion.1) | copy-start | bytes 1572868
Sparse Core Ops, SparseCore 0:
  8.9 25.2 all-gather.9
  35.8 72.0 all-gather.11
  109.5 70.6 all-gather.13
  181.6 70.6 all-gather.15
  262.1 29.7 reduce-scatter.3
  294.1 22.5 all-gather.17
  318.2 45.6 all-gather.21
  365.5 44.4 all-gather.19
  411.5 44.4 all-gather.23
  462.6 29.9 reduce-scatter.5
  494.8 22.5 all-gather.25
  535.1 31.1 reduce-scatter.7
where the time goes:
time: 576 us; the launch traced here: 575 us
  waiting for transfers between devices  495 us (86%)
  matrix products  42.7 us (7%)
  other arithmetic  14.1 us (2%)
  between operations  13.7 us (2%)
  blocking collectives  6.51 us (1%)
    all_gather x1, waiting for transfers between devices, half_again(): lax.all_gather(proj_down, 'fs', axis=1, tiled=True)  72.1 us
    all_gather x1, waiting for transfers between devices, half_again(): lax.all_gather(proj_gate, 'fs', axis=0, tiled=True)  71.5 us
    all_gather x1, waiting for transfers between devices, half_again(): lax.all_gather(proj_lift, 'fs', axis=0, tiled=True)  66.6 us
    reduce_scatter x2, waiting for transfers between devices, half_again(): lax.psum_scatter(partial_value.astype(jnp.bfloat16), 'tp', scatter_dimens...  61.2 us
    all_gather x2, waiting for transfers between devices, gathered_norm(): gathered = lax.all_gather(stream_rows, 'tp', axis=0, tiled=True)  47.3 us
    all_gather x1, waiting for transfers between devices, token_mixer(): lax.all_gather(mixer_down, 'fs', axis=1, tiled=True)  46.1 us
    all_gather x1, waiting for transfers between devices, token_mixer(): lax.all_gather(mixer_v, 'fs', axis=0, tiled=True)  45 us
    all_gather x1, waiting for transfers between devices, token_mixer(): lax.all_gather(mixer_u, 'fs', axis=0, tiled=True)  30.2 us
  transfers between devices with their start and end apart: 12, of which 12 were waited for; matrix products, arithmetic and copies ran while one was open for 3% of the time, Pallas kernels for 0%

commit v1 on v0

--- a/solution.py
+++ b/solution.py
@@ -8,6 +8,24 @@
 A = 2048
 norm_epsilon = 1e-06
 layer_epsilon = 1e-05
+
+
+def collect(array, axis, dim):
+    ways, here, step = (lax.axis_size(axis), lax.axis_index(axis), array.shape[dim])
+    shape = [n * ways if d == dim else n for d, n in enumerate(array.shape)]
+    full = lax.dynamic_update_slice_in_dim(
+        jnp.zeros(shape, array.dtype), array, here * step, axis=dim
+    )
+    going_up = going_down = array
+    for far in range(1, ways // 2 + 1):
+        going_up = lax.ppermute(going_up, axis, [(d, (d + 1) % ways) for d in range(ways)])
+        full = lax.dynamic_update_slice_in_dim(full, going_up, (here - far) % ways * step, axis=dim)
+        if 2 * far < ways:
+            going_down = lax.ppermute(going_down, axis, [(d, (d - 1) % ways) for d in range(ways)])
+            full = lax.dynamic_update_slice_in_dim(
+                full, going_down, (here + far) % ways * step, axis=dim
+            )
+    return full
 
 
 def norm_rows(row_block, scale_gain):
@@ -35,11 +53,7 @@
 def half_again(stream_rows, scale_gain, proj_gate, proj_lift, proj_down):
     normed = gathered_norm(stream_rows, scale_gain)
     gate_vals, lift_vals = pair_adder(
-        normed,
-        (
-            lax.all_gather(proj_gate, "fs", axis=0, tiled=True),
-            lax.all_gather(proj_lift, "fs", axis=0, tiled=True),
-        ),
+        normed, (lax.all_gather(proj_gate, "fs", axis=0, tiled=True), collect(proj_lift, "fs", 0))
     )
     hidden = activate(gate_vals, lift_vals)
     partial_value = jnp.dot(

time: 576 us -> 529 us (0.918)
  waiting for transfers between devices: 495 us -> 436 us
  local copies, waits for them, and re-layouts: 2.34 us -> 9.91 us
    ppermute x0 -> x3, waiting for transfers between devices: none -> 79.1 us  [the longest x2 45.6 us: collect(): lax.ppermute(going_up, axis, [(d, (d + 1) % ways) for d in range(ways)])]
    all_gather x1 -> x0, waiting for transfers between devices: 66.6 us -> none  [half_again(): lax.all_gather(proj_lift, 'fs', axis=0, tiled=True)]
    all_gather x1, waiting for transfers between devices: 71.5 us -> 30.3 us  [half_again(): lax.all_gather(proj_gate, 'fs', axis=0, tiled=True)]
    all_gather x2, waiting for transfers between devices: 47.3 us -> 22.7 us  [gathered_norm(): gathered = lax.all_gather(stream_rows, 'tp', axis=0, tiled=True)]
  transfers between devices with their start and end apart: 12 -> 14, of which waited for: 12 -> 13; matrix products, arithmetic and copies ran while one was open for 3% -> 5% of each run, Pallas kernels for 0% -> 0%
where the time goes in v1:
time: 529 us; the launch traced here: 528 us
  waiting for transfers between devices  436 us (82%)
  matrix products  42.7 us (8%)
  other arithmetic  14.1 us (3%)
  between operations  13.3 us (3%)
  local copies, waits for them, and re-layouts  9.91 us (2%)
  blocking collectives  6.69 us (1%)
  starting transfers between devices  5.6 us (1%)
    all_gather x1, waiting for transfers between devices, half_again(): lax.all_gather(proj_down, 'fs', axis=1, tiled=True)  67.2 us
    reduce_scatter x2, waiting for transfers between devices, half_again(): lax.psum_scatter(partial_value.astype(jnp.bfloat16), 'tp', scatter_dimens...  61.2 us
    all_gather x1, waiting for transfers between devices, token_mixer(): lax.all_gather(mixer_down, 'fs', axis=1, tiled=True)  46.1 us
    ppermute x2, waiting for transfers between devices, collect(): lax.ppermute(going_up, axis, [(d, (d + 1) % ways) for d in range(ways)])  45.6 us
    all_gather x1, waiting for transfers between devices, token_mixer(): lax.all_gather(mixer_v, 'fs', axis=0, tiled=True)  44.9 us
    ppermute x1, waiting for transfers between devices, collect(): lax.ppermute(going_down, axis, [(d, (d - 1) % ways) for d in range(ways)])  33.4 us
    all_gather x1, waiting for transfers between devices, half_again(): lax.all_gather(proj_gate, 'fs', axis=0, tiled=True)  30.3 us
    reduce_scatter x1, waiting for transfers between devices, token_mixer(): lax.psum_scatter(partial_value.astype(jnp.bfloat16), 'tp', scatter_dimens...  30.1 us
  transfers between devices with their start and end apart: 14, of which 13 were waited for; matrix products, arithmetic and copies ran while one was open for 5% of the time, Pallas kernels for 0%

profile of v1, /device:TPU:0, one launch (start us, length us, event | category | flops | bytes accessed | tf_op | source)
XLA Modules:
  0.0 528.4 jit_solution(1927523975750392994)
XLA Ops:
  6.5 0.7 all-gather.9.cloned.1.call-update
  7.3 0.0 all-gather.11.cloned.1.call-start
  7.3 0.7 all-gather.11.cloned.1.call-update
  8.0 0.0 all-gather.13.cloned.1.call-start
  8.1 0.7 all-gather.13.cloned.1.call-update
  8.7 0.0 reduce-scatter.4.cloned.1.call-start
  8.8 3.1 collective-permute-start
  11.9 2.1 collective-permute-start.1
  14.0 21.2 %collective-permute-done = bf16[512,896]{1,0:T(8,128)(2,1)S(1)} collective-permute-done((bf16[512,896]{1,0:T(8,128)(2,1)S(1)}, bf16[512,896]{1,0:T(8,128)(2,1)S(1)}, u32[]{:S(2)}, u32[]{:S(2)}) %collective-permute-start) | collective-permute-done | bytes 917536 | tf_op jit(solution)/shard_map/ppermute | solution.py:21
  35.2 0.0 collective-permute-start.2
  35.2 2.2 broadcast.77
  37.4 1.1 constant_dynamic-update-slice_fusion.3
  38.4 1.0 constant_dynamic-update-slice_fusion.2
  39.5 33.4 %collective-permute-done.1 = bf16[512,896]{1,0:T(8,128)(2,1)} collective-permute-done((bf16[512,896]{1,0:T(8,128)(2,1)S(1)}, bf16[512,896]{1,0:T(8,128)(2,1)}, u32[]{:S(2)}, u32[]{:S(2)}) %collective-permute-start.1) | collective-permute-done | bytes 917536 | tf_op jit(solution)/shard_map/ppermute | solution.py:24
  72.9 2.3 constant_dynamic-update-slice_fusion.1
  75.2 24.5 %collective-permute-done.2 = bf16[512,896]{1,0:T(8,128)(2,1)S(1)} collective-permute-done((bf16[512,896]{1,0:T(8,128)(2,1)S(1)}, bf16[512,896]{1,0:T(8,128)(2,1)S(1)}, u32[]{:S(2)}, u32[]{:S(2)}) %collective-permute-start.2) | collective-permute-done | bytes 917536 | tf_op jit(solution)/shard_map/ppermute | solution.py:21
  99.6 1.0 constant_dynamic-update-slice_fusion
  100.6 2.2 fusion
  102.9 30.3 %all-gather.11.cloned.1.call-done = bf16[2048,896]{1,0:T(8,128)(2,1)} async-done(((bf16[512,896]{1,0:T(8,128)(2,1)}), bf16[2048,896]{1,0:T(8,128)(2,1)}) %all-gather.11.cloned.1.call-update) | async-done | bytes 3670032 | tf_op jit(solution)/shard_map/all_gather | solution.py:56
  133.2 5.6 %fusion.42 = f32[512,896]{1,0:T(8,128)} fusion(bf16[2048,896]{1,0:T(8,128)(2,1)} %all-gather.11.cloned.1.call-done, bf16[512,2048]{1,0:T(8,128)(2,1)S(1)} %copy-done.3, f32[2048]{0:T(1024)S(1)} %copy-done.11, f32[512]{0:T(512)S(1)} %add_rsqrt_fusion.3), kind=kOutput, calls=%fused_computation.48 | convolution fusion | flops 1883242496 | bytes 7612416 | tf_op jit(solution)/shard_map/dot_general | solution.py:44
  138.8 67.2 %all-gather.13.cloned.1.call-done = bf16[896,2048]{1,0:T(8,128)(2,1)} async-done(((bf16[896,512]{1,0:T(8,128)(2,1)}), bf16[896,2048]{1,0:T(8,128)(2,1)}) %all-gather.13.cloned.1.call-update) | async-done | bytes 3670032 | tf_op jit(solution)/shard_map/all_gather | solution.py:61
  206.0 9.7 %convolution_convert_fusion.1 = bf16[512,2048]{1,0:T(8,128)(2,1)} fusion(bf16[896,2048]{1,0:T(8,128)(2,1)} %all-gather.13.cloned.1.call-done, f32[512,896]{1,0:T(8,128)} %fusion.42, bf16[2048,896]{1,0:T(8,128)(2,1)} %constant_dynamic-update-slice_fusion, bf16[512,2048]{1,0:T(8,128)(2,1)S(1)} %copy-done.3, f32[2048]{0:T(1024)S(1)} %copy-done.11, ...), kind=kOutput, calls=%fused_computation.16 | convolution fusion | flops 3766091776 | bytes 13379584 | tf_op jit(solution)/shard_map/dot_general | solution.py:59
  215.7 0.0 reduce-scatter.4.cloned.1.call-update
  215.7 0.0 all-gather.15.cloned.1.call-start
  215.8 29.8 %reduce-scatter.4.cloned.1.call-done = bf16[128,2048]{1,0:T(8,128)(2,1)} async-done(((bf16[512,2048]{1,0:T(8,128)(2,1)}), bf16[128,2048]{1,0:T(8,128)(2,1)}) %reduce-scatter.4.cloned.1.call-update) | async-done | bytes 524304 | tf_op jit(solution)/shard_map/reduce_scatter | solution.py:64
  245.6 0.0 copy-done.2
  245.6 2.0 add_convert_fusion.3
  247.6 0.0 all-gather.15.cloned.1.call-update
  247.6 0.0 all-gather.19.cloned.1.call-start
  247.7 0.5 all-gather.19.cloned.1.call-update
  248.2 0.0 all-gather.17.cloned.1.call-start
  248.2 0.7 all-gather.17.cloned.1.call-update
  248.9 0.0 all-gather.21.cloned.1.call-start
  249.0 0.7 all-gather.21.cloned.1.call-update
  249.7 0.0 reduce-scatter.6.cloned.1.call-start
  249.8 20.6 %all-gather.15.cloned.1.call-done = bf16[512,2048]{1,0:T(8,128)(2,1)} async-done(((bf16[128,2048]{1,0:T(8,128)(2,1)}), bf16[512,2048]{1,0:T(8,128)(2,1)}) %all-gather.15.cloned.1.call-update) | async-done | bytes 2097168 | tf_op jit(solution)/shard_map/all_gather | solution.py:81
  270.3 2.2 fusion.3
  272.6 0.0 copy-start.8
  272.6 0.0 copy-start.9
  272.6 44.9 %all-gather.19.cloned.1.call-done = bf16[2048,512]{1,0:T(8,128)(2,1)} async-done(((bf16[512,512]{1,0:T(8,128)(2,1)}), bf16[2048,512]{1,0:T(8,128)(2,1)}) %all-gather.19.cloned.1.call-update) | async-done | bytes 2097168 | tf_op jit(solution)/shard_map/all_gather | solution.py:88
  317.5 4.2 fusion.60
  321.6 6.7 %all-reduce = (f32[512]{0:T(512)S(1)}, f32[512]{0:T(512)S(1)}) all-reduce(f32[512]{0:T(512)S(1)} %get-tuple-element.6, f32[512]{0:T(512)S(1)} %get-tuple-element.5), channel_id=1, replica_groups=mesh['rep'=2,'fs'=4,'tp'=4] {'tp'}, use_global_device_ids=true, to_apply=%region_6.7 | all-reduce | flops 1024 | bytes 8192 | tf_op jit(solution)/shard_map/psum | solution.py:92
  328.3 1.5 add_convert_fusion.2
  329.8 0.9 reshape.47
  330.7 0.0 copy-done.7
  330.7 1.4 fusion.9
  332.1 1.4 copy.21
  333.5 30.0 %all-gather.17.cloned.1.call-done = bf16[2048,512]{1,0:T(8,128)(2,1)} async-done(((bf16[512,512]{1,0:T(8,128)(2,1)}), bf16[2048,512]{1,0:T(8,128)(2,1)}) %all-gather.17.cloned.1.call-update) | async-done | bytes 2097168 | tf_op jit(solution)/shard_map/all_gather | solution.py:87
  363.5 46.1 %all-gather.21.cloned.1.call-done = bf16[512,2048]{1,0:T(8,128)(2,1)} async-done(((bf16[512,512]{1,0:T(8,128)(2,1)}), bf16[512,2048]{1,0:T(8,128)(2,1)}) %all-gather.21.cloned.1.call-update) | async-done | bytes 2097168 | tf_op jit(solution)/shard_map/all_gather | solution.py:110
  409.6 6.5 %convolution_convert_fusion.2 = bf16[512,2048]{1,0:T(8,128)(2,1)} fusion(bf16[512,2048]{1,0:T(8,128)(2,1)} %all-gather.21.cloned.1.call-done, f32[64,8,4,128]{3,2,1,0:T(4,128)} %bitcast.25, bf16[2048,512]{1,0:T(8,128)(2,1)} %all-gather.17.cloned.1.call-done, bf16[512,2048]{1,0:T(8,128)(2,1)S(1)} %copy-done.4, f32[2048]{0:T(1024)S(1)} %copy-done.12, ...), kind=kOutput, calls=%fused_computation.17 | convolution fusion | flops 2155347968 | bytes 9447424 | tf_op jit(solution)/shard_map/dot_general | solution.py:108
  416.1 0.0 reduce-scatter.6.cloned.1.call-update
  416.1 0.0 copy-start.13
  416.1 0.0 all-gather.23.cloned.1.call-start
  416.1 30.1 %reduce-scatter.6.cloned.1.call-done = bf16[128,2048]{1,0:T(8,128)(2,1)} async-done(((bf16[512,2048]{1,0:T(8,128)(2,1)}), bf16[128,2048]{1,0:T(8,128)(2,1)}) %reduce-scatter.6.cloned.1.call-update) | async-done | bytes 524304 | tf_op jit(solution)/shard_map/reduce_scatter | solution.py:113
  446.2 2.0 add_convert_fusion.1
  448.2 0.0 all-gather.23.cloned.1.call-update
  448.2 0.0 reduce-scatter.8.cloned.1.call-start
  448.3 22.7 %all-gather.23.cloned.1.call-done = bf16[512,2048]{1,0:T(8,128)(2,1)} async-done(((bf16[128,2048]{1,0:T(8,128)(2,1)}), bf16[512,2048]{1,0:T(8,128)(2,1)}) %all-gather.23.cloned.1.call-update) | async-done | bytes 2097168 | tf_op jit(solution)/shard_map/all_gather | solution.py:38
  470.9 2.2 fusion.6
  473.2 5.7 %fusion.28 = f32[512,896]{1,0:T(8,128)} fusion(bf16[2048,896]{1,0:T(8,128)(2,1)} %all-gather.11.cloned.1.call-done, bf16[512,2048]{1,0:T(8,128)(2,1)S(1)} %copy-done.5, f32[2048]{0:T(1024)S(1)} %copy-done.13, f32[512]{0:T(512)S(1)} %add_rsqrt_fusion), kind=kOutput, calls=%fused_computation.45 | convolution fusion | flops 1883242496 | bytes 7612416 | tf_op jit(solution)/shard_map/dot_general | solution.py:44
  478.9 9.6 %convolution_convert_fusion = bf16[512,2048]{1,0:T(8,128)(2,1)} fusion(bf16[896,2048]{1,0:T(8,128)(2,1)} %all-gather.13.cloned.1.call-done, f32[512,896]{1,0:T(8,128)} %fusion.28, bf16[2048,896]{1,0:T(8,128)(2,1)} %constant_dynamic-update-slice_fusion, bf16[512,2048]{1,0:T(8,128)(2,1)S(1)} %copy-done.5, f32[2048]{0:T(1024)S(1)} %copy-done.13, ...), kind=kOutput, calls=%fused_computation.15 | convolution fusion | flops 3766091776 | bytes 13379584 | tf_op jit(solution)/shard_map/dot_general | solution.py:59
  488.5 0.0 reduce-scatter.8.cloned.1.call-update
  488.5 31.3 %reduce-scatter.8.cloned.1.call-done = bf16[128,2048]{1,0:T(8,128)(2,1)} async-done(((bf16[512,2048]{1,0:T(8,128)(2,1)}), bf16[128,2048]{1,0:T(8,128)(2,1)}) %reduce-scatter.8.cloned.1.call-update) | async-done | bytes 524304 | tf_op jit(solution)/shard_map/reduce_scatter | solution.py:64
  519.9 2.0 add_convert_fusion
  (30 shorter events, 0.1 us)
Async XLA Ops:
  6.5 2.3 copy-start.6
  6.5 94.1 %all-gather.9.cloned.1.call-start = ((), (), s32[]{:S(2)}) async-start(), calls=%async_computation.3 | async-start | bytes 2621440 | tf_op jit(solution)/shard_map/all_gather | solution.py:38
  7.3 125.9 %all-gather.11.cloned.1.call-start = ((), (), s32[]{:S(2)}) async-start(), calls=%async_computation.4 | async-start | bytes 4587520 | tf_op jit(solution)/shard_map/all_gather | solution.py:56
  8.0 198.0 %all-gather.13.cloned.1.call-start = ((), (), s32[]{:S(2)}) async-start(), calls=%async_computation.5 | async-start | bytes 4587520 | tf_op jit(solution)/shard_map/all_gather | solution.py:61
  8.7 236.8 %reduce-scatter.4.cloned.1.call-start = ((), (), s32[]{:S(2)}) async-start(), calls=%async_computation.6 | async-start | bytes 2621440 | tf_op jit(solution)/shard_map/reduce_scatter | solution.py:64
  8.8 26.4 %collective-permute-start = (bf16[512,896]{1,0:T(8,128)(2,1)S(1)}, bf16[512,896]{1,0:T(8,128)(2,1)S(1)}, u32[]{:S(2)}, u32[]{:S(2)}) collective-permute-start(bf16[512,896]{1,0:T(8,128)(2,1)S(1)} %copy-done.6), channel_id=1, source_target_pairs={{0,4},{4,8},{8,12},{12,0},{1,5},{5,9},{9,13},{13,1},{2,6},{6,10},{... | collective-permute-start | bytes 2752520 | tf_op jit(solution)/shard_map/ppermute | solution.py:21
  11.9 61.0 %collective-permute-start.1 = (bf16[512,896]{1,0:T(8,128)(2,1)S(1)}, bf16[512,896]{1,0:T(8,128)(2,1)}, u32[]{:S(2)}, u32[]{:S(2)}) collective-permute-start(bf16[512,896]{1,0:T(8,128)(2,1)S(1)} %copy-done.6), channel_id=1, source_target_pairs={{0,12},{4,0},{8,4},{12,8},{1,13},{5,1},{9,5},{13,9},{2,14},{6,2},{... | collective-permute-start | bytes 2752520 | tf_op jit(solution)/shard_map/ppermute | solution.py:24
  35.2 64.4 %collective-permute-start.2 = (bf16[512,896]{1,0:T(8,128)(2,1)S(1)}, bf16[512,896]{1,0:T(8,128)(2,1)S(1)}, u32[]{:S(2)}, u32[]{:S(2)}) collective-permute-start(bf16[512,896]{1,0:T(8,128)(2,1)S(1)} %collective-permute-done), channel_id=1, source_target_pairs={{0,4},{4,8},{8,12},{12,0},{1,5},{5,9},{9,13},{13,1},{2,6},{6,10},{... | collective-permute-start | bytes 2752520 | tf_op jit(solution)/shard_map/ppermute | solution.py:21
  75.2 58.0 %copy-start.11 = (f32[2048]{0:T(1024)S(1)}, f32[2048]{0:T(1024)}, u32[]{:S(2)}) copy-start(f32[2048]{0:T(1024)} %param.15) | copy-start | bytes 24580
  100.6 32.6 %copy-start.3 = (bf16[512,2048]{1,0:T(8,128)(2,1)S(1)}, bf16[512,2048]{1,0:T(8,128)(2,1)}, u32[]{:S(2)}) copy-start(bf16[512,2048]{1,0:T(8,128)(2,1)} %all-gather.9.cloned.1.call-done) | copy-start | bytes 6291460
  215.7 29.9 %copy-start.2 = (bf16[128,2048]{1,0:T(8,128)(2,1)S(1)}, bf16[128,2048]{1,0:T(8,128)(2,1)}, u32[]{:S(2)}) copy-start(bf16[128,2048]{1,0:T(8,128)(2,1)} %param.14) | copy-start | bytes 1572868
  215.7 54.6 %all-gather.15.cloned.1.call-start = ((), (), s32[]{:S(2)}) async-start(), calls=%async_computation.7 | async-start | bytes 2621440 | tf_op jit(solution)/shard_map/all_gather | solution.py:81
  247.6 69.9 %copy-start.12 = (f32[2048]{0:T(1024)S(1)}, f32[2048]{0:T(1024)}, u32[]{:S(2)}) copy-start(f32[2048]{0:T(1024)} %param.20) | copy-start | bytes 24580
  247.6 69.8 %all-gather.19.cloned.1.call-start = ((), (), s32[]{:S(2)}) async-start(), calls=%async_computation.9 | async-start | bytes 2621440 | tf_op jit(solution)/shard_map/all_gather | solution.py:88
  248.2 115.3 %all-gather.17.cloned.1.call-start = ((), (), s32[]{:S(2)}) async-start(), calls=%async_computation.8 | async-start | bytes 2621440 | tf_op jit(solution)/shard_map/all_gather | solution.py:87
  248.9 160.6 %all-gather.21.cloned.1.call-start = ((), (), s32[]{:S(2)}) async-start(), calls=%async_computation.10 | async-start | bytes 2621440 | tf_op jit(solution)/shard_map/all_gather | solution.py:110
  249.7 196.5 %reduce-scatter.6.cloned.1.call-start = ((), (), s32[]{:S(2)}) async-start(), calls=%async_computation.11 | async-start | bytes 2621440 | tf_op jit(solution)/shard_map/reduce_scatter | solution.py:113
  270.3 47.1 %copy-start.4 = (bf16[512,2048]{1,0:T(8,128)(2,1)S(1)}, bf16[512,2048]{1,0:T(8,128)(2,1)}, u32[]{:S(2)}) copy-start(bf16[512,2048]{1,0:T(8,128)(2,1)} %all-gather.15.cloned.1.call-done) | copy-start | bytes 6291460
  272.6 55.7 %copy-start.8 = (f32[512]{0:T(512)S(1)}, f32[512]{0:T(512)}, u32[]{:S(2)}) copy-start(f32[512]{0:T(512)} %param.24) | copy-start | bytes 6148
  272.6 55.7 %copy-start.9 = (f32[512]{0:T(512)S(1)}, f32[512]{0:T(512)}, u32[]{:S(2)}) copy-start(f32[512]{0:T(512)} %param.23) | copy-start | bytes 6148
  321.6 9.1 %copy-start.7 = (bf16[4,128,128]{2,1,0:T(8,128)(2,1)S(1)}, bf16[4,128,128]{2,1,0:T(8,128)(2,1)}, u32[]{:S(2)}) copy-start(bf16[4,128,128]{2,1,0:T(8,128)(2,1)} %param.25) | copy-start | bytes 393220
  321.6 9.1 %copy-start.10 = (f32[4,128]{1,0:T(4,128)S(1)}, f32[4,128]{1,0:T(4,128)}, u32[]{:S(2)}) copy-start(f32[4,128]{1,0:T(4,128)} %param.26) | copy-start | bytes 6148
  416.1 30.2 %copy-start = (bf16[128,2048]{1,0:T(8,128)(2,1)S(1)}, bf16[128,2048]{1,0:T(8,128)(2,1)}, u32[]{:S(2)}) copy-start(bf16[128,2048]{1,0:T(8,128)(2,1)} %add_convert_fusion.3) | copy-start | bytes 1572868
  416.1 57.1 %copy-start.13 = (f32[2048]{0:T(1024)S(1)}, f32[2048]{0:T(1024)}, u32[]{:S(2)}) copy-start(f32[2048]{0:T(1024)} %param.16) | copy-start | bytes 24580
  416.1 54.8 %all-gather.23.cloned.1.call-start = ((), (), s32[]{:S(2)}) async-start(), calls=%async_computation.12 | async-start | bytes 2621440 | tf_op jit(solution)/shard_map/all_gather | solution.py:38
  448.2 71.7 %reduce-scatter.8.cloned.1.call-start = ((), (), s32[]{:S(2)}) async-start(), calls=%async_computation.13 | async-start | bytes 2621440 | tf_op jit(solution)/shard_map/reduce_scatter | solution.py:64
  470.9 2.2 copy-start.5
  488.5 31.4 %copy-start.1 = (bf16[128,2048]{1,0:T(8,128)(2,1)S(1)}, bf16[128,2048]{1,0:T(8,128)(2,1)}, u32[]{:S(2)}) copy-start(bf16[128,2048]{1,0:T(8,128)(2,1)} %add_convert_fusion.1) | copy-start | bytes 1572868
Sparse Core Ops, SparseCore 0:
  8.9 25.2 all-gather.8
  35.8 97.3 all-gather.10
  134.8 71.1 all-gather.12
  215.8 29.7 reduce-scatter.3
  247.7 22.5 all-gather.14
  271.8 45.6 all-gather.18
  319.0 44.4 all-gather.16
  365.1 44.4 all-gather.20
  416.2 29.9 reduce-scatter.5
  448.3 22.5 all-gather.22
  488.6 31.1 reduce-scatter.7
